TPU v7x, 32 devices: a whole 2x2x4 slice. The times are simulated.
32 devices in a mesh: grp: 2 (over y), sp: 4 (over z), tp: 4 (over x, core).
Axes of the slice: x: 2, y: 2, z: 4, core: 2. Of those that a mesh axis runs over, the one named last changes fastest.
Arguments:
- tokens: bfloat16 [4096, 2048], P(('grp', 'sp')), parts along dimension 0, may hold values from -6 to 6
- fresh_token_input: bfloat16 [4096], P('grp'), parts along dimension 0, may hold values from -6 to 6
- value_matrix: bfloat16 [2048, 2048], P(None, 'tp'), may hold values from -0.125 to 0.125
- write_matrix: bfloat16 [2048, 1024], P(None, 'tp'), may hold values from -0.125 to 0.125
- read_matrix: bfloat16 [2048, 1024], P(None, 'tp'), may hold values from -0.125 to 0.125
- gate_matrix: bfloat16 [2048, 2048], P(None, 'tp'), may hold values from -0.125 to 0.125
- step_matrix: bfloat16 [2048, 32], replicated, may hold values from -0.125 to 0.125
- value_filter_taps: bfloat16 [4, 2048], replicated, may hold values from -3 to 3
- write_filter_taps: bfloat16 [4, 1024], replicated, may hold values from -3 to 3
- read_filter_taps: bfloat16 [4, 1024], replicated, may hold values from -3 to 3
- head_log_decay: float32 [32], replicated
- step_offset_bias: float32 [32], replicated, may hold values from -3.5 to -2.5
- decay_spike: float32 [4096, 32], P(('grp', 'sp'), 'tp'), parts along dimension 0, may hold values from -3 to 0, as said below
- bypass_scale: float32 [32], replicated, may hold values from 0.5 to 2
- group_norm_scale: float32 [2048], replicated, may hold values from 0.1 to 1.9
Outputs:
- prompt_out: bfloat16 [4096, 2048], P(('grp', 'sp'), 'tp'), parts along dimension 0
- state_cache: bfloat16 [256, 2048], P(('grp', 'sp'), 'tp'), parts along dimension 0
- step_out: bfloat16 [1024, 4], P(('grp', 'tp'), 'sp'), parts along dimension 0
There are 2 independent parts, one for each index of `grp`. A program takes and returns all parts, laid end to end along the dimension named above; an argument that names none is the same for every part. Nothing has to cross between parts.
Inputs may be any that keep to these rules, and one draw needn't show every extreme that they name: `decay_spike`: never positive.
All inputs are finite; a program needn't handle non-finite values.
Results may differ from a plain program's by a relative error of at most 0.023.
Values may be sent and summed in bfloat16 or wider, within the bound.
A program may use at most 64 MiB of HBM per device.

v0:
```python
import jax
import jax.numpy as jnp
from jax import lax
from jax.sharding import PartitionSpec as P

HEAD = 64
STATE = 128
CONV = 4
BLOCK = 128


epsilon = 1e-06


def passed_along(block, axis, distance):
    devices = range(lax.axis_size(axis))
    route = [(i - distance, i) for i in devices if i - distance in devices]
    return lax.ppermute(block, axis, route)


def from_root(value, axis, source):
    kept = jnp.where(lax.axis_index(axis) == source, value, 0).astype(value.dtype)
    return lax.psum(kept, axis)


def project(operand, weights):
    return jnp.dot(operand, weights, preferred_element_type=jnp.float32).astype(jnp.bfloat16)


def apply_taps(previous, current, tap_weights):
    joined = jnp.concatenate([previous, current], axis=0).astype(jnp.float32)
    length = current.shape[0]
    summed = jnp.zeros(current.shape, jnp.float32)
    for offset in range(CONV):
        summed = summed + tap_weights[offset].astype(jnp.float32) * joined[offset : offset + length]
    return summed


def group_norm(gated_rows, groups):
    shaped = gated_rows.reshape(gated_rows.shape[:-1] + (groups, -1))
    normed = shaped * lax.rsqrt(jnp.mean(shaped * shaped, axis=-1, keepdims=True) + epsilon)
    return normed.reshape(gated_rows.shape)


def read_new(cached, stored_portion, read_part, new_decay, step_now, value_now):
    states = cached.astype(jnp.float32).reshape((cached.shape[0],) + value_now.shape)
    updated = (
        new_decay[None, :, :, None] * states
        + step_now[None, :, :, None] * stored_portion.T[:, :, None, None] * value_now[None]
    )
    return jnp.einsum("gn,ngep->gep", read_part, updated, precision=lax.Precision.HIGHEST)


def on_device(
    tokens,
    fresh_token_input,
    value_matrix,
    write_matrix,
    read_matrix,
    gate_matrix,
    step_matrix,
    value_filter_taps,
    write_filter_taps,
    read_filter_taps,
    head_log_decay,
    step_offset_bias,
    decay_spike,
    bypass_scale,
    group_norm_scale,
):
    head_rank = lax.axis_index("tp")
    sequence_rank = lax.axis_index("sp")
    sequence_count = lax.axis_size("sp")
    channels = value_matrix.shape[1]
    head_count = channels // HEAD
    map_width = write_matrix.shape[1]
    group_count = map_width // STATE
    per_group = head_count // group_count
    row_count = tokens.shape[0]
    head_start = head_rank * head_count
    local_count = STATE // sequence_count
    own_step = lax.dynamic_slice_in_dim(step_matrix, head_start, head_count, 1)
    own_value_taps = lax.dynamic_slice_in_dim(value_filter_taps, head_rank * channels, channels, 1)
    own_write_taps = lax.dynamic_slice_in_dim(
        write_filter_taps, head_rank * map_width, map_width, 1
    )
    own_read_taps = lax.dynamic_slice_in_dim(read_filter_taps, head_rank * map_width, map_width, 1)
    head_decay_rates = jnp.exp(lax.dynamic_slice_in_dim(head_log_decay, head_start, head_count, 0))
    own_bias = lax.dynamic_slice_in_dim(step_offset_bias, head_start, head_count, 0)
    own_skip = lax.dynamic_slice_in_dim(bypass_scale, head_start, head_count, 0)
    own_gain = lax.dynamic_slice_in_dim(group_norm_scale, head_rank * channels, channels, 0)
    value_rows = project(tokens, value_matrix)
    write_rows = project(tokens, write_matrix)
    read_rows = project(tokens, read_matrix)
    gate_rows = project(tokens, gate_matrix)
    step_raw = jnp.dot(tokens, own_step, preferred_element_type=jnp.float32)
    edge = row_count - (CONV - 1)
    tail_rows = (value_rows[edge:], write_rows[edge:], read_rows[edge:])
    before = passed_along((tail_rows[0], tail_rows[1], tail_rows[2]), "sp", 1)
    ending = (
        from_root(tail_rows[0], "sp", sequence_count - 1),
        from_root(tail_rows[1], "sp", sequence_count - 1),
        from_root(tail_rows[2], "sp", sequence_count - 1),
    )
    values = jax.nn.silu(apply_taps(before[0], value_rows, own_value_taps)).astype(jnp.bfloat16)
    writes = jax.nn.silu(apply_taps(before[1], write_rows, own_write_taps)).astype(jnp.bfloat16)
    reads = jax.nn.silu(apply_taps(before[2], read_rows, own_read_taps)).astype(jnp.bfloat16)
    step_length = jax.nn.softplus(step_raw + own_bias)
    log_decay_value = decay_spike - step_length * head_decay_rates
    blocks = row_count // BLOCK
    block_values = values.reshape(blocks, BLOCK, group_count, per_group, HEAD)
    block_writes = writes.reshape(blocks, BLOCK, group_count, STATE)
    block_reads = reads.reshape(blocks, BLOCK, group_count, STATE)
    block_steps = step_length.reshape(blocks, BLOCK, group_count, per_group)
    cumulative = jnp.cumsum(log_decay_value.reshape(blocks, BLOCK, group_count, per_group), axis=1)
    block_end = cumulative[:, -1]
    scaled = (
        (jnp.exp(block_end[:, None] - cumulative) * block_steps)[..., None]
        * block_values.astype(jnp.float32)
    ).astype(jnp.bfloat16)
    block_states = jnp.einsum(
        "bsgn,bsgep->bngep", block_writes, scaled, preferred_element_type=jnp.float32
    )
    running = jnp.zeros((STATE, group_count, per_group, HEAD), jnp.float32)
    inside = []
    for block_index in range(blocks):
        inside.append(running)
        running = (
            jnp.exp(block_end[block_index])[None, :, :, None] * running + block_states[block_index]
        )
    local_states = jnp.stack(inside)
    shard_fading_factor = jnp.sum(block_end, axis=0)
    before_block = jnp.cumsum(block_end, axis=0) - block_end
    decay_table = lax.all_gather(shard_fading_factor[None], "sp", axis=0, tiled=True)
    inclusive = jnp.cumsum(decay_table, axis=0)
    exclusive = inclusive - decay_table
    total_decay = inclusive[-1]
    row_pieces = lax.all_to_all(running[None], "sp", split_axis=1, concat_axis=0, tiled=True)
    ranks = jnp.arange(sequence_count)
    below = (ranks[None, :] < ranks[:, None])[:, :, None, None]
    prefix_weight = jnp.exp(jnp.where(below, exclusive[:, None] - inclusive[None, :], -jnp.inf))
    prefix_rows = jnp.einsum(
        "jkge,kngep->jngep", prefix_weight, row_pieces, precision=lax.Precision.HIGHEST
    )
    final_weight = jnp.exp(total_decay[None] - inclusive)
    final_rows = jnp.einsum(
        "kge,kngep->ngep", final_weight, row_pieces, precision=lax.Precision.HIGHEST
    )
    earlier_state = lax.all_to_all(prefix_rows, "sp", split_axis=0, concat_axis=1, tiled=True)[0]
    scores = jnp.einsum(
        "blgn,bsgn->bgls", block_reads, block_writes, preferred_element_type=jnp.float32
    )
    cum_heads = jnp.transpose(cumulative, (0, 2, 3, 1))
    decay_gaps = cum_heads[..., :, None] - cum_heads[..., None, :]
    step_heads = jnp.transpose(block_steps, (0, 2, 3, 1))
    causal = jnp.tril(jnp.ones((BLOCK, BLOCK), bool))
    mixing = (
        scores[:, :, None]
        * jnp.exp(jnp.where(causal, decay_gaps, -jnp.inf))
        * step_heads[..., None, :]
    ).astype(jnp.bfloat16)
    inner_part = jnp.einsum(
        "bgels,bsgep->blgep", mixing, block_values, preferred_element_type=jnp.float32
    )
    entering = jnp.exp(before_block)[:, None, :, :, None] * earlier_state[None] + local_states
    carried_part = jnp.exp(cumulative)[..., None] * jnp.einsum(
        "blgn,bngep->blgep",
        block_reads.astype(jnp.float32),
        entering,
        precision=lax.Precision.HIGHEST,
    )
    mixed_rows = (inner_part + carried_part).reshape(row_count, head_count, HEAD) + own_skip[
        None, :, None
    ] * values.astype(jnp.float32).reshape(row_count, head_count, HEAD)
    gated_rows = mixed_rows.reshape(row_count, channels) * jax.nn.silu(
        gate_rows.astype(jnp.float32)
    )
    prompt_out = (group_norm(gated_rows, group_count) * own_gain).astype(jnp.bfloat16)
    new_row = fresh_token_input[None]
    new_value = project(new_row, value_matrix)
    new_write = project(new_row, write_matrix)
    new_read = project(new_row, read_matrix)
    new_gate = project(new_row, gate_matrix)
    new_step = jax.nn.softplus(
        jnp.dot(new_row, own_step, preferred_element_type=jnp.float32)[0] + own_bias
    )
    new_values = jax.nn.silu(apply_taps(ending[0], new_value, own_value_taps)).astype(jnp.bfloat16)
    latest_stores = jax.nn.silu(apply_taps(ending[1], new_write, own_write_taps)).astype(
        jnp.bfloat16
    )
    new_reads = jax.nn.silu(apply_taps(ending[2], new_read, own_read_taps)).astype(jnp.bfloat16)
    value_now = new_values.astype(jnp.float32).reshape(group_count, per_group, HEAD)
    write_now = latest_stores.astype(jnp.float32).reshape(group_count, STATE)
    read_now = new_reads.astype(jnp.float32).reshape(group_count, STATE)
    new_decay = jnp.exp(-new_step * head_decay_rates).reshape(group_count, per_group)
    step_now = new_step.reshape(group_count, per_group)
    row_start = sequence_rank * local_count
    cache_rows = final_rows.reshape(local_count, channels).astype(jnp.bfloat16)
    stored_portion = lax.dynamic_slice_in_dim(write_now, row_start, local_count, 1)
    read_part = lax.dynamic_slice_in_dim(read_now, row_start, local_count, 1)
    partial_value = read_new(cache_rows, stored_portion, read_part, new_decay, step_now, value_now)
    reading = lax.psum(partial_value, "sp")
    new_mixed = reading + own_skip.reshape(group_count, per_group)[:, :, None] * value_now
    new_gated = new_mixed.reshape(1, channels) * jax.nn.silu(new_gate.astype(jnp.float32))
    step_whole = (group_norm(new_gated, group_count) * own_gain).astype(jnp.bfloat16)[0]
    step_table = step_whole.reshape(channels // sequence_count, sequence_count)
    step_out = lax.dynamic_slice_in_dim(step_table, sequence_rank, 1, 1)
    return (prompt_out, cache_rows, step_out)


def solution(mesh):
    placed = (
        P(("grp", "sp"), None),
        P("grp"),
        P(None, "tp"),
        P(None, "tp"),
        P(None, "tp"),
        P(None, "tp"),
        P(),
        P(),
        P(),
        P(),
        P(),
        P(),
        P(("grp", "sp"), "tp"),
        P(),
        P(),
    )
    return jax.shard_map(
        on_device,
        mesh=mesh,
        in_specs=placed,
        out_specs=(P(("grp", "sp"), "tp"), P(("grp", "sp"), "tp"), P(("grp", "tp"), "sp")),
        check_vma=False,
    )
```

profile of v0, /device:TPU:0, one launch (start us, length us, event | category | flops | bytes accessed | tf_op | source)
XLA Modules:
  0.0 126.4 jit_solution(4960432107386798171)
XLA Ops:
  0.7 1.6 %copy-done = bf16[512,2048]{1,0:T(8,128)(2,1)S(1)} copy-done((bf16[512,2048]{1,0:T(8,128)(2,1)S(1)}, bf16[512,2048]{1,0:T(8,128)(2,1)}, u32[]{:S(2)}) %copy-start) | copy-done | bytes 2097176
  2.2 1.9 %convolution_convert_fusion.2 = bf16[512,256]{1,0:T(8,128)(2,1)S(1)} fusion(bf16[512,2048]{1,0:T(8,128)(2,1)S(1)} %copy-done, bf16[2048,256]{1,0:T(8,128)(2,1)} %param.18), kind=kOutput, calls=%fused_computation.11 | convolution fusion | flops 537001984 | bytes 3407872 | tf_op jit(solution)/shard_map/dot_general | solution.py:27
  4.2 0.6 broadcast_select_fusion.1
  4.7 5.7 %collective-permute-start.2 = (bf16[3,256]{1,0:T(4,128)(2,1)}, bf16[3,256]{1,0:T(4,128)(2,1)}, u32[]{:S(2)}, u32[]{:S(2)}) collective-permute-start(bf16[3,256]{1,0:T(4,128)(2,1)} %get-tuple-element.57), channel_id=1, source_target_pairs={{0,4},{4,8},{8,12},{1,5},{5,9},{9,13},{2,6},{6,10},{10,14},{3,7},{... | collective-permute-start | bytes 4616 | tf_op jit(solution)/shard_map/ppermute | solution.py:18
  10.4 0.7 convolution_convert_fusion.3
  11.1 0.6 fusion.92
  11.8 3.6 %collective-permute-start.1 = (bf16[3,256]{1,0:T(4,128)(2,1)}, bf16[3,256]{1,0:T(4,128)(2,1)}, u32[]{:S(2)}, u32[]{:S(2)}) collective-permute-start(bf16[3,256]{1,0:T(4,128)(2,1)} %get-tuple-element.54), channel_id=1, source_target_pairs={{0,4},{4,8},{8,12},{1,5},{5,9},{9,13},{2,6},{6,10},{10,14},{3,7},{... | collective-permute-start | bytes 4616 | tf_op jit(solution)/shard_map/ppermute | solution.py:18
  15.4 1.3 convolution_convert_fusion.1
  16.7 0.8 copy-done.8
  17.5 0.6 fusion.91
  18.1 3.5 %collective-permute-start = (bf16[3,512]{1,0:T(4,128)(2,1)}, bf16[3,512]{1,0:T(4,128)(2,1)}, u32[]{:S(2)}, u32[]{:S(2)}) collective-permute-start(bf16[3,512]{1,0:T(4,128)(2,1)} %get-tuple-element.52), channel_id=1, source_target_pairs={{0,4},{4,8},{8,12},{1,5},{5,9},{9,13},{2,6},{6,10},{10,14},{3,7},{... | collective-permute-start | bytes 9224 | tf_op jit(solution)/shard_map/ppermute | solution.py:18
  21.6 0.5 iota_compare_fusion.1
  22.4 1.5 %fusion.96 = f32[1,256]{1,0:T(1,128)S(1)} fusion(bf16[2048,1]{0,1:T(2,128)(2,1)S(1)} %reshape.251, bf16[2048,256]{1,0:T(8,128)(2,1)} %param.19), kind=kOutput, calls=%fused_computation.194 | convolution fusion | flops 1048576 | bytes 1053696 | tf_op jit(solution)/shard_map/dot_general | solution.py:27
  24.5 0.7 multiply_exponential_fusion
  25.1 0.7 multiply_subtract_fusion
  26.3 0.6 fusion.76
  27.1 2.0 %fusion.99 = f32[1,512]{1,0:T(1,128)S(1)} fusion(bf16[2048,1]{0,1:T(2,128)(2,1)S(1)} %reshape.251, bf16[2048,512]{1,0:T(8,128)(2,1)} %param.20), kind=kOutput, calls=%fused_computation.197 | convolution fusion | flops 2097152 | bytes 2103296 | tf_op jit(solution)/shard_map/dot_general | solution.py:27
  29.1 7.6 %all-gather.1 = f32[4,2,4]{2,1,0:T(2,128)S(1)} all-gather(f32[1,2,4]{2,1,0:T(2,128)S(1)} %bitcast.152), channel_id=2, replica_groups=mesh['grp'=2,'sp'=4,'tp'=4] {'sp'}, dimensions={0}, use_global_device_ids=true | all-gather | bytes 160 | tf_op jit(solution)/shard_map/all_gather | solution.py:134
  36.7 10.5 %all-reduce = (bf16[3,512]{1,0:T(4,128)(2,1)S(1)}, bf16[3,256]{1,0:T(4,128)(2,1)S(1)}, bf16[3,256]{1,0:T(4,128)(2,1)S(1)}) all-reduce(bf16[3,512]{1,0:T(4,128)(2,1)S(1)} %get-tuple-element.53, bf16[3,256]{1,0:T(4,128)(2,1)S(1)} %get-tuple-element.56, ...), channel_id=1, replica_groups=mesh['grp'=2,'sp'=4,'tp'=4] {'sp'}, use_global_device_ids=true, to_apply=%region_7.8 | all-reduce | flops 3072 | bytes 12288 | tf_op jit(solution)/shard_map/psum | solution.py:23
  47.3 0.7 convert_convert_fusion
  48.1 1.0 copy.149
  49.2 0.7 convert_reduce_fusion.1
  49.9 2.4 %fusion.90 = (f32[4,128,2,4]{3,2,1,0:T(2,128)}, f32[4,128,2,4]{3,2,1,0:T(2,128)S(1)}) fusion(f32[4,128,2,4]{3,2,1,0:T(2,128)S(1)} %fusion.94, f32[4,128,2,4]{3,2,1,0:T(2,128)} %copy.149, f32[4,2,4]{2,1,0:T(2,128)S(1)} %get-tuple-element.47), kind=kLoop, calls=%fused_computation.187 | loop fusion | flops 8192 | bytes 65664 | tf_op jit(solution)/shard_map/exp | solution.py:166
  52.4 0.7 convert_reduce_fusion
  53.0 0.6 fusion.81
  53.7 0.7 dynamic_slice.39
  54.5 0.7 mul.552
  55.2 0.7 mul.510
  55.9 1.3 %mul.529 = f32[2,4]{1,0:T(2,128)} reshape(f32[8]{0:T(128)} %get-tuple-element.28) | data formatting | bytes 64 | tf_op jit(solution)/shard_map/mul | solution.py:48
  57.6 1.3 %copy.148 = f32[4,128,2,4]{1,3,2,0:T(4,128)S(1)} copy(f32[4,128,2,4]{3,2,1,0:T(2,128)} %get-tuple-element.44) | data formatting | bytes 32768 | tf_op jit(solution)/shard_map/exp | solution.py:166
  59.1 0.6 pad.6.clone
  59.7 0.7 maximum_convert_fusion.2
  60.5 1.0 multiply_convert_fusion.5
  61.5 0.8 maximum_convert_fusion.1
  62.8 0.8 maximum_convert_fusion
  63.6 1.3 %multiply_convert_fusion.4 = bf16[512,512]{1,0:T(8,128)(2,1)S(1)} fusion(f32[515,512]{1,0:T(8,128)S(1)} %maximum_convert_fusion, f32[512]{0:T(512)} %bitcast.141, f32[512]{0:T(512)} %bitcast.140, f32[512]{0:T(512)S(1)} %bitcast.139, f32[512]{0:T(512)S(1)} %bitcast.138), kind=kLoop, calls=%fused_computation.44 | loop fusion | flops 3145728 | bytes 4726784 | tf_op jit(solution)/shard_map/convert_element_type | solution.py:105
  65.0 1.0 copy.140
  66.0 2.0 %reshape.229 = bf16[4,128,2,4,64]{1,0,4,3,2:T(4,128)(2,1)} reshape(bf16[512,512]{0,1:T(8,128)(2,1)} %copy.140) | data formatting | bytes 1048576 | tf_op jit(solution)/shard_map/reshape | solution.py:111
  68.0 1.3 multiply_convert_fusion.3
  69.5 1.0 slice_add_fusion
  70.8 1.2 reshape.274
  72.0 3.6 %all-to-all-start = ((f32[4,1,16384]{2,1,0:T(1,128)}), f32[4,1,16384]{2,1,0:T(1,128)S(1)}, u32[]{:S(2)}, u32[]{:S(2)}) async-start(f32[4,1,16384]{2,1,0:T(1,128)} %reshape.274), calls=%async_computation | async-start | bytes 524288 | tf_op jit(solution)/shard_map/all_to_all | solution.py:138
  75.9 3.0 %convolution_bitcast_fusion.2 = f32[4,128,2,4,64]{1,4,3,2,0:T(8,128)} fusion(f32[4,2,4,128]{3,2,1,0:T(4,128)S(1)} %copy.146, f32[4,2,4,128]{3,2,1,0:T(4,128)S(1)} %copy.144, f32[4,2,128,128]{3,2,1,0:T(8,128)S(1)} %fusion.40, pred[128,128]{1,0:T(8,128)(4,1)S(1)} %iota_compare_fusion, bf16[4,128,2,4,64]{1,0,4,3,2:T(4,128)(2,1)} %reshape.229), kind=kOutput, calls=%fused_computation.5 | convolution fusion | flops 69730304 | bytes 2146304 | tf_op jit(solution)/shard_map/bgels,bsgep->blgep/dot_general | solution.py:162
  78.8 3.3 %all-to-all-done = f32[4,1,16384]{2,1,0:T(1,128)S(1)} async-done(((f32[4,1,16384]{2,1,0:T(1,128)}), f32[4,1,16384]{2,1,0:T(1,128)S(1)}, u32[]{:S(2)}, u32[]{:S(2)}) %all-to-all-start) | async-done | bytes 262176 | tf_op jit(solution)/shard_map/all_to_all | solution.py:138
  82.1 0.5 broadcast.118
  82.7 1.3 %reduce.9 = f32[4,16384]{1,0:T(4,128)S(1)} reduce(f32[4,1,16384]{2,1,0:T(1,128)S(1)} %all-to-all-done, f32[]{:T(128)} %broadcast.118), dimensions={1}, to_apply=%all_to_all.6.reduce_sub_computation | reduce | bytes 524292 | tf_op jit(solution)/shard_map/all_to_all | solution.py:138
  84.4 1.3 %fusion.35 = bf16[2,4,1,32,64]{4,2,3,1,0:T(2,128)(2,1)S(1)} fusion(f32[4,2,4,1,1]{0,3,4,2,1:T(1,128)S(1)} %copy.173, f32[4,32,2,4,64]{4,3,2,1,0:T(4,128)S(1)} %bitcast.123), kind=kOutput, calls=%fused_computation.69 | convolution fusion | flops 786432 | bytes 295040 | tf_op jit(solution)/shard_map/kge,kngep->ngep/dot_general | solution.py:146
  85.7 1.3 %convolution_bitcast_fusion.3 = f32[4,32,2,4,64]{4,0,1,3,2:T(4,128)S(1)} fusion(f32[4,32,2,4,64]{4,3,2,1,0:T(4,128)S(1)} %bitcast.124, f32[4,2,4]{0,2,1:T(4,128)S(1)} %copy.156, f32[4,2,4]{0,2,1:T(4,128)S(1)} %copy.155, pred[4,4]{1,0:T(4,128)(4,1)S(1)} %copy-done.30), kind=kOutput, calls=%fused_computation.10 | convolution fusion | flops 3145984 | bytes 524560 | tf_op jit(solution)/shard_map/jkge,kngep->jngep/dot_general | solution.py:142
  87.1 1.0 reshape.276
  88.1 3.4 %all-to-all-start.1 = ((f32[4,1,16384]{2,1,0:T(1,128)}), f32[4,1,16384]{2,1,0:T(1,128)S(1)}, u32[]{:S(2)}, u32[]{:S(2)}) async-start(f32[4,1,16384]{2,1,0:T(1,128)} %reshape.276), calls=%async_computation.1 | async-start | bytes 524288 | tf_op jit(solution)/shard_map/all_to_all | solution.py:149
  91.9 12.2 %psum.31 = f32[2,4,64]{2,1,0:T(4,128)S(1)} all-reduce(f32[2,4,64]{2,1,0:T(4,128)S(1)} %bitcast.137), channel_id=1, replica_groups=mesh['grp'=2,'sp'=4,'tp'=4] {'sp'}, use_global_device_ids=true, to_apply=%region_8.9 | all-reduce | flops 512 | bytes 4096 | tf_op jit(solution)/shard_map/psum | solution.py:202
  104.5 0.7 convert_element_type.211
  105.3 0.8 multiply_convert_fusion.7
  106.3 0.6 copy.168
  106.9 1.3 %reduce.10 = f32[4,16384]{1,0:T(4,128)S(1)} reduce(f32[4,1,16384]{2,1,0:T(1,128)S(1)} %all-to-all-done.1, f32[]{:T(128)} %broadcast.118), dimensions={1}, to_apply=%all_to_all.8.reduce_sub_computation | reduce | bytes 524292 | tf_op jit(solution)/shard_map/all_to_all | solution.py:149
  108.5 0.9 copy.160
  109.4 2.3 %fusion.1 = f32[4,128,2,4,64]{1,4,3,2,0:T(8,128)S(1)} fusion(f32[4,128,2,4,64]{1,4,3,2,0:T(8,128)} %convolution_bitcast_fusion.2, f32[1,128,2,4,64]{1,4,3,2,0:T(8,128)} %get-tuple-element.41, f32[1,128,2,4,64]{1,4,3,2,0:T(8,128)} %get-tuple-element.42, f32[1,128,2,4,64]{1,4,3,2,0:T(8,128)} %get-tuple-element.43, f32[4]{0:T(128)S(1)} %copy-done.31, ...), kind=kOutput, calls=%fused_computation.4 | convolution fusion | flops 404488192 | bytes 3424400 | tf_op jit(solution)/shard_map/blgn,bngep->blgep/dot_general | solution.py:166
  111.7 1.8 %copy.184 = f32[4,128,2,4,64]{4,3,2,1,0:T(4,128)} copy(f32[4,128,2,4,64]{1,4,3,2,0:T(8,128)S(1)} %fusion.1) | data formatting | bytes 2097152 | tf_op jit(solution)/shard_map/reshape | solution.py:172
  113.5 3.5 %reshape.263 = f32[512,512]{1,0:T(8,128)} reshape(f32[4,128,2,4,64]{4,3,2,1,0:T(4,128)} %copy.184) | data formatting | bytes 2097152 | tf_op jit(solution)/shard_map/reshape | solution.py:172
  117.0 4.6 %fusion.93 = (f32[512,512]{1,0:T(8,128)}, f32[512,512]{1,0:T(8,128)}) fusion(bf16[512,2048]{1,0:T(8,128)(2,1)S(1)} %copy-done, bf16[2048,512]{1,0:T(8,128)(2,1)} %param.20, f32[512,512]{1,0:T(8,128)} %reshape.263, bf16[512,512]{1,0:T(8,128)(2,1)S(1)} %copy-done.2, f32[512]{0:T(512)S(1)} %copy-done.25), kind=kOutput, calls=%fused_computation.190 | convolution fusion | flops 1076625408 | bytes 7866368 | tf_op jit(solution)/shard_map/dot_general | solution.py:27
  121.7 1.9 %mul.516 = f32[512,2,256]{2,1,0:T(2,128)S(1)} reshape(f32[512,512]{1,0:T(8,128)} %get-tuple-element.63) | data formatting | bytes 2097152 | tf_op jit(solution)/shard_map/mul | solution.py:41
  123.5 0.6 reduce_sum.28
  124.2 0.6 mul.517
  125.4 1.1 multiply_convert_fusion.2
  (128 shorter events, 6.4 us)
Async XLA Ops:
  0.6 1.6 %copy-start = (bf16[512,2048]{1,0:T(8,128)(2,1)S(1)}, bf16[512,2048]{1,0:T(8,128)(2,1)}, u32[]{:S(2)}) copy-start(bf16[512,2048]{1,0:T(8,128)(2,1)} %param.15) | copy-start | bytes 6291460
  0.6 9.8 %copy-start.6 = (bf16[2048,256]{1,0:T(8,128)(2,1)S(1)}, bf16[2048,256]{1,0:T(8,128)(2,1)}, u32[]{:S(2)}) copy-start(bf16[2048,256]{1,0:T(8,128)(2,1)} %param.19) | copy-start | bytes 3145732
  4.2 11.3 %copy-start.3 = (bf16[2048,512]{1,0:T(8,128)(2,1)S(1)}, bf16[2048,512]{1,0:T(8,128)(2,1)}, u32[]{:S(2)}) copy-start(bf16[2048,512]{1,0:T(8,128)(2,1)} %param.17) | copy-start | bytes 6291460
  4.7 55.0 %collective-permute-start.2 = (bf16[3,256]{1,0:T(4,128)(2,1)}, bf16[3,256]{1,0:T(4,128)(2,1)}, u32[]{:S(2)}, u32[]{:S(2)}) collective-permute-start(bf16[3,256]{1,0:T(4,128)(2,1)} %get-tuple-element.57), channel_id=1, source_target_pairs={{0,4},{4,8},{8,12},{1,5},{5,9},{9,13},{2,6},{6,10},{10,14},{3,7},{... | collective-permute-start | bytes 4616 | tf_op jit(solution)/shard_map/ppermute | solution.py:18
  11.1 0.7 copy-start.10
  11.8 10.3 %copy-start.23 = (bf16[2048]{0:T(1024)(128)(2,1)S(1)}, bf16[2048]{0:T(1024)(128)(2,1)}, u32[]{:S(2)}) copy-start(bf16[2048]{0:T(1024)(128)(2,1)} %param.16) | copy-start | bytes 12292
  11.8 10.3 %copy-start.5 = (bf16[2048,256]{1,0:T(8,128)(2,1)S(1)}, bf16[2048,256]{1,0:T(8,128)(2,1)}, u32[]{:S(2)}) copy-start(bf16[2048,256]{1,0:T(8,128)(2,1)} %param.18) | copy-start | bytes 3145732
  11.8 49.6 %collective-permute-start.1 = (bf16[3,256]{1,0:T(4,128)(2,1)}, bf16[3,256]{1,0:T(4,128)(2,1)}, u32[]{:S(2)}, u32[]{:S(2)}) collective-permute-start(bf16[3,256]{1,0:T(4,128)(2,1)} %get-tuple-element.54), channel_id=1, source_target_pairs={{0,4},{4,8},{8,12},{1,5},{5,9},{9,13},{2,6},{6,10},{10,14},{3,7},{... | collective-permute-start | bytes 4616 | tf_op jit(solution)/shard_map/ppermute | solution.py:18
  16.7 0.8 copy-start.8
  18.1 44.7 %collective-permute-start = (bf16[3,512]{1,0:T(4,128)(2,1)}, bf16[3,512]{1,0:T(4,128)(2,1)}, u32[]{:S(2)}, u32[]{:S(2)}) collective-permute-start(bf16[3,512]{1,0:T(4,128)(2,1)} %get-tuple-element.52), channel_id=1, source_target_pairs={{0,4},{4,8},{8,12},{1,5},{5,9},{9,13},{2,6},{6,10},{10,14},{3,7},{... | collective-permute-start | bytes 9224 | tf_op jit(solution)/shard_map/ppermute | solution.py:18
  21.6 2.3 %copy-start.4 = (bf16[2048,512]{1,0:T(8,128)(2,1)S(1)}, bf16[2048,512]{1,0:T(8,128)(2,1)}, u32[]{:S(2)}) copy-start(bf16[2048,512]{1,0:T(8,128)(2,1)} %param.17) | copy-start | bytes 6291460
  22.1 2.2 %copy-start.33 = (f32[32]{0:T(128)S(1)}, f32[32]{0:T(128)}, u32[]{:S(2)}) copy-start(f32[32]{0:T(128)} %param.26) | copy-start | bytes 388
  22.2 2.3 %copy-start.32 = (f32[32]{0:T(128)S(1)}, f32[32]{0:T(128)}, u32[]{:S(2)}) copy-start(f32[32]{0:T(128)} %param.25) | copy-start | bytes 388
  22.2 3.0 %copy-start.12 = (f32[512,8]{0,1:T(8,128)S(1)}, f32[512,8]{0,1:T(8,128)}, u32[]{:S(2)}) copy-start(f32[512,8]{0,1:T(8,128)} %param.27) | copy-start | bytes 49156
  22.4 2.0 %copy-start.13 = (bf16[2048,32]{0,1:T(8,128)(2,1)S(1)}, bf16[2048,32]{0,1:T(8,128)(2,1)}, u32[]{:S(2)}) copy-start(bf16[2048,32]{0,1:T(8,128)(2,1)} %param.21) | copy-start | bytes 393220
  25.8 21.5 %copy-start.26 = (bf16[4,1024]{1,0:T(4,128)(2,1)S(1)}, bf16[4,1024]{1,0:T(4,128)(2,1)}, u32[]{:S(2)}) copy-start(bf16[4,1024]{1,0:T(4,128)(2,1)} %param.23) | copy-start | bytes 24580
  26.1 23.0 %copy-start.27 = (bf16[4,1024]{1,0:T(4,128)(2,1)S(1)}, bf16[4,1024]{1,0:T(4,128)(2,1)}, u32[]{:S(2)}) copy-start(bf16[4,1024]{1,0:T(4,128)(2,1)} %param.24) | copy-start | bytes 24580
  27.1 25.3 %copy-start.22 = (bf16[4,2048]{1,0:T(4,128)(2,1)S(1)}, bf16[4,2048]{1,0:T(4,128)(2,1)}, u32[]{:S(2)}) copy-start(bf16[4,2048]{1,0:T(4,128)(2,1)} %param.22) | copy-start | bytes 49156
  57.6 3.9 %copy-start.11 = (bf16[512,256]{1,0:T(8,128)(2,1)S(1)}, bf16[512,256]{1,0:T(8,128)(2,1)}, u32[]{:S(2)}) copy-start(bf16[512,256]{1,0:T(8,128)(2,1)} %copy-done.10) | copy-start | bytes 786436
  59.1 3.1 %copy-start.18 = (f32[1,256]{1,0:T(1,128)S(1)}, f32[1,256]{1,0:T(1,128)}, u32[]{:S(2)}) copy-start(f32[1,256]{1,0:T(1,128)} %get-tuple-element.24) | copy-start | bytes 3076
  59.1 3.2 %copy-start.19 = (f32[1,256]{1,0:T(1,128)S(1)}, f32[1,256]{1,0:T(1,128)}, u32[]{:S(2)}) copy-start(f32[1,256]{1,0:T(1,128)} %get-tuple-element.25) | copy-start | bytes 3076
  59.1 3.2 %copy-start.20 = (f32[1,256]{1,0:T(1,128)S(1)}, f32[1,256]{1,0:T(1,128)}, u32[]{:S(2)}) copy-start(f32[1,256]{1,0:T(1,128)} %get-tuple-element.26) | copy-start | bytes 3076
  59.1 3.2 %copy-start.21 = (f32[1,256]{1,0:T(1,128)S(1)}, f32[1,256]{1,0:T(1,128)}, u32[]{:S(2)}) copy-start(f32[1,256]{1,0:T(1,128)} %get-tuple-element.27) | copy-start | bytes 3076
  61.5 1.3 %copy-start.9 = (bf16[512,512]{1,0:T(8,128)(2,1)S(1)}, bf16[512,512]{1,0:T(8,128)(2,1)}, u32[]{:S(2)}) copy-start(bf16[512,512]{1,0:T(8,128)(2,1)} %copy-done.8) | copy-start | bytes 1572868
  65.0 4.5 %copy-start.1 = (bf16[512,512]{1,0:T(8,128)(2,1)}, bf16[512,512]{1,0:T(8,128)(2,1)S(1)}, u32[]{:S(2)}) copy-start(bf16[512,512]{1,0:T(8,128)(2,1)S(1)} %multiply_convert_fusion.4) | copy-start | bytes 1572868
  66.0 3.5 %copy-start.14 = (f32[2,4]{1,0:T(2,128)S(1)}, f32[2,4]{1,0:T(2,128)}, u32[]{:S(2)}) copy-start(f32[2,4]{1,0:T(2,128)} %get-tuple-element.48) | copy-start | bytes 100
  66.0 3.5 %copy-start.15 = (f32[2,4]{1,0:T(2,128)S(1)}, f32[2,4]{1,0:T(2,128)}, u32[]{:S(2)}) copy-start(f32[2,4]{1,0:T(2,128)} %get-tuple-element.49) | copy-start | bytes 100
  68.0 1.6 %copy-start.16 = (f32[2,4]{1,0:T(2,128)S(1)}, f32[2,4]{1,0:T(2,128)}, u32[]{:S(2)}) copy-start(f32[2,4]{1,0:T(2,128)} %get-tuple-element.50) | copy-start | bytes 100
  68.0 1.6 %copy-start.17 = (f32[2,4]{1,0:T(2,128)S(1)}, f32[2,4]{1,0:T(2,128)}, u32[]{:S(2)}) copy-start(f32[2,4]{1,0:T(2,128)} %get-tuple-element.51) | copy-start | bytes 100
  72.0 10.2 %all-to-all-start = ((f32[4,1,16384]{2,1,0:T(1,128)}), f32[4,1,16384]{2,1,0:T(1,128)S(1)}, u32[]{:S(2)}, u32[]{:S(2)}) async-start(f32[4,1,16384]{2,1,0:T(1,128)} %reshape.274), calls=%async_computation | async-start | bytes 524288 | tf_op jit(solution)/shard_map/all_to_all | solution.py:138
  75.9 9.8 %copy-start.30 = (pred[4,4]{1,0:T(4,128)(4,1)S(1)}, pred[4,4]{1,0:T(4,128)(4,1)}, u32[]{:S(2)}) copy-start(pred[4,4]{1,0:T(4,128)(4,1)} %iota_compare_fusion.1) | copy-start | bytes 52
  84.3 7.2 %copy-start.28 = (f32[2,4]{1,0:T(2,128)S(1)}, f32[2,4]{1,0:T(2,128)}, u32[]{:S(2)}) copy-start(f32[2,4]{1,0:T(2,128)} %mul.529) | copy-start | bytes 100
  84.3 7.4 %copy-start.24 = (bf16[2,32,1,1]{1,0,2,3:T(2,128)(2,1)S(1)}, bf16[2,32,1,1]{1,0,2,3:T(2,128)(2,1)}, u32[]{:S(2)}) copy-start(bf16[2,32,1,1]{1,0,2,3:T(2,128)(2,1)} %fusion.81) | copy-start | bytes 388
  85.7 18.4 %copy-start.29 = (f32[2,4]{1,0:T(2,128)S(1)}, f32[2,4]{1,0:T(2,128)}, u32[]{:S(2)}) copy-start(f32[2,4]{1,0:T(2,128)} %mul.552) | copy-start | bytes 100
  88.1 18.8 %all-to-all-start.1 = ((f32[4,1,16384]{2,1,0:T(1,128)}), f32[4,1,16384]{2,1,0:T(1,128)S(1)}, u32[]{:S(2)}, u32[]{:S(2)}) async-start(f32[4,1,16384]{2,1,0:T(1,128)} %reshape.276), calls=%async_computation.1 | async-start | bytes 524288 | tf_op jit(solution)/shard_map/all_to_all | solution.py:149
  91.5 17.9 %copy-start.31 = (f32[4]{0:T(128)S(1)}, f32[4]{0:T(128)}, u32[]{:S(2)}) copy-start(f32[4]{0:T(128)} %pad.6.clone) | copy-start | bytes 52
  113.5 3.5 %copy-start.2 = (bf16[512,512]{1,0:T(8,128)(2,1)S(1)}, bf16[512,512]{1,0:T(8,128)(2,1)}, u32[]{:S(2)}) copy-start(bf16[512,512]{1,0:T(8,128)(2,1)} %copy-done.1) | copy-start | bytes 1572868
  113.5 3.5 %copy-start.25 = (f32[512]{0:T(512)S(1)}, f32[512]{0:T(512)}, u32[]{:S(2)}) copy-start(f32[512]{0:T(512)} %mul.510) | copy-start | bytes 6148
  124.2 1.2 copy-start.7
where the time goes:
time: 127 us; the launch traced here: 126 us
  blocking collectives  30.3 us (24%)
  local copies, waits for them, and re-layouts  28.8 us (23%)
  matrix products  22.6 us (18%)
  other arithmetic  20.4 us (16%)
  starting transfers between devices  19.8 us (16%)
  waiting for transfers between devices  3.3 us (3%)
    ppermute x3, starting transfers between devices, passed_along(): return lax.ppermute(block, axis, route)  12.8 us
    dot_general x8, matrix products, project(): jnp.dot(operand, weights, preferred_element_type=jnp.float32)  12.6 us
    psum x1, blocking collectives, on_device(): reading = lax.psum(partial_value, 'sp')  12.2 us
    psum x1, blocking collectives, from_root(): return lax.psum(kept, axis)  10.5 us
    all_gather x1, blocking collectives, on_device(): lax.all_gather(shard_fading_factor[None], 'sp', axis=0, tiled=True)  7.58 us
    unnamed x75, local copies, waits for them, and re-layouts  6.63 us
    reshape x2, local copies, waits for them, and re-layouts, on_device(): (inner_part + carried_part).reshape(row_count, head_count, HEAD)  5.28 us
    all_to_all x1, starting transfers between devices, on_device(): lax.all_to_all(running[None], 'sp', split_axis=1, concat_axis=0, tiled=True)  3.58 us
  transfers between devices with their start and end apart: 5, of which 1 were waited for; matrix products, arithmetic and copies ran while one was open for 26% of the time, Pallas kernels for 0%

commit v1 on v0

v1 whole, which is shorter than its diff:
```python
import functools

import jax
import jax.numpy as jnp
from jax import lax
from jax.experimental import pallas as pl
from jax.experimental.pallas import tpu as pltpu
from jax.sharding import PartitionSpec as P

HEAD = 64
STATE = 128
CONV = 4
BLOCK = 128
PAD = 16
LANES = 128
EPSILON = 1e-06
F32 = jnp.float32
BF16 = jnp.bfloat16
MESH = pl.DeviceIdType.MESH


def dot(a, b, dims=((1,), (0,)), precision=None):
    return lax.dot_general(a, b, (dims, ((), ())), precision=precision, preferred_element_type=F32)


def silu(x):
    half = 0.5 * x
    return half + half * jnp.tanh(half)


def softplus(x):
    return jnp.maximum(x, 0.0) + jnp.log1p(jnp.exp(-jnp.abs(x)))


def split(x):
    high = x.astype(BF16)
    return jnp.concatenate([high.astype(F32), x - high.astype(F32)], axis=0).astype(BF16)


def kernel(
    n, tokens, fresh, w_value, w_write, w_read, w_gate, step_t, taps_v, taps_w, taps_r,
    log_rate, offset_bias, spike_t, bypass, gain,
    out, cache_out, step_out,
    xs, wv, ww, wr, wg, pv, pw, pr, pg, raw_t, vals, wrt, rds, y_loc, fade, local_state,
    received, sending, cache, step_row, step_recv, result,
    load_sem, halo_send, halo_recv, chain_send, chain_recv, cache_send, cache_recv,
    row_send, row_recv, out_sem,
):
    rows, width = tokens.shape
    channels = w_value.shape[1]
    maps = w_write.shape[1]
    groups = maps // STATE
    heads = channels // HEAD
    per_group = heads // groups
    wide = per_group * HEAD
    blocks = rows // BLOCK
    all_heads = step_t.shape[0]
    piece = STATE // n
    tp = lax.axis_index("tp")
    me = lax.axis_index("sp")
    last = n - 1
    chunks = channels // LANES
    chunks_group = wide // LANES

    loads = []

    def load(src, dst):
        copy = pltpu.make_async_copy(src, dst, load_sem.at[len(loads)])
        loads.append(copy)
        copy.start()
        return copy

    get_tokens = load(tokens, xs.at[pl.ds(PAD, rows)])
    get_gate = [load(w_gate.at[:, pl.ds(g * wide, wide)], wg.at[:, pl.ds(g * wide, wide)]) for g in range(groups)]
    get_write = load(w_write, ww)
    get_value = [load(w_value.at[:, pl.ds(g * wide, wide)], wv.at[:, pl.ds(g * wide, wide)]) for g in range(groups)]
    get_read = load(w_read, wr)

    barrier = pltpu.get_barrier_semaphore()

    @pl.when(me > 0)
    def _():
        pl.semaphore_signal(barrier, inc=1, device_id={"sp": me - 1}, device_id_type=MESH)

    @pl.when(me < last)
    def _():
        pl.semaphore_wait(barrier, 1)

    following = jnp.minimum(me + 1, last)
    halo = pltpu.make_async_remote_copy(
        src_ref=tokens.at[pl.ds(rows - PAD, PAD)], dst_ref=xs.at[pl.ds(0, PAD)],
        send_sem=halo_send, recv_sem=halo_recv, device_id={"sp": following}, device_id_type=MESH,
    )

    @pl.when(me < last)
    def _():
        halo.start()

    fresh_f = fresh[...].astype(F32)
    fresh_row = jnp.concatenate([fresh_f[i : i + 1] for i in range(width // LANES)], axis=1)
    xs[pl.ds(PAD + rows, PAD)] = jnp.broadcast_to(fresh_row, (PAD, width)).astype(BF16)

    @pl.when(me == 0)
    def _():
        xs[pl.ds(0, PAD)] = jnp.zeros((PAD, width), BF16)

    lane = lax.broadcasted_iota(jnp.int32, (heads, all_heads), 1)
    own = lane == lax.broadcasted_iota(jnp.int32, (heads, all_heads), 0) + tp * heads

    def column(ref):
        return jnp.sum(jnp.where(own, ref[...], 0.0), axis=1, keepdims=True)

    rates = jnp.exp(column(log_rate))
    bias = column(offset_bias)
    expand = (
        lax.broadcasted_iota(jnp.int32, (heads, channels), 1) // HEAD
        == lax.broadcasted_iota(jnp.int32, (heads, channels), 0)
    ).astype(F32)
    expand2 = jnp.concatenate([expand, expand], axis=0).astype(BF16)

    def spread(x):
        return dot(split(x), expand2, ((0,), (0,)))

    skip_row = jnp.sum(expand * column(bypass), axis=0, keepdims=True)
    gain_row = jnp.concatenate(
        [gain[pl.ds(tp * (channels // LANES) + i, 1)] for i in range(channels // LANES)], axis=1
    )

    get_tokens.wait()
    raw = dot(xs[pl.ds(PAD, rows + PAD)], step_t[...], ((1,), (1,)))
    raw_t[...] = raw[:rows].T
    if heads % 8 == 0:
        own_raw = raw_t[pl.ds(pl.multiple_of(tp * heads, 8), heads)]
    else:
        own_raw = dot(own.astype(F32), raw_t[...], precision=lax.Precision.HIGHEST)
    raw_new = jnp.sum(jnp.where(own, raw[rows : rows + 1], 0.0), axis=1, keepdims=True)
    step = softplus(own_raw + bias)
    new_step = softplus(raw_new + bias)
    log_decay = spike_t[...] - step * rates
    upper = (
        lax.broadcasted_iota(jnp.int32, (BLOCK, BLOCK), 0)
        <= lax.broadcasted_iota(jnp.int32, (BLOCK, BLOCK), 1)
    ).astype(F32)
    cums = [
        dot(log_decay[:, k * BLOCK : (k + 1) * BLOCK], upper, precision=lax.Precision.HIGHEST)
        for k in range(blocks)
    ]
    ends = [c[:, BLOCK - 1 :] for c in cums]
    before = [jnp.zeros_like(ends[0])]
    for k in range(blocks):
        before.append(before[k] + ends[k])
    scale_in = jnp.concatenate([jnp.exp(ends[k] - cums[k]) for k in range(blocks)], axis=1) * step
    cum_cols = [c.T for c in cums]
    end_rows = [jnp.sum(expand * jnp.exp(e), axis=0, keepdims=True) for e in ends]
    total_row = jnp.sum(expand * jnp.exp(before[blocks]), axis=0, keepdims=True)

    for g in range(groups):
        cols = pl.ds(g * wide, wide)
        get_gate[g].wait()
        pg[:, cols] = dot(xs[pl.ds(PAD, rows + PAD)], wg[:, cols])

    @pl.when(me > 0)
    def _():
        halo.wait_recv()

    def conv(src, taps, base, cols, start, count):
        own_cols = pl.ds(pl.multiple_of(base + cols.start, LANES), cols.size)
        weights = taps[:, own_cols].astype(F32)
        total = None
        for k in range(CONV):
            term = weights[k : k + 1] * src[pl.ds(start - (CONV - 1) + k, count), cols]
            total = term if total is None else total + term
        return silu(total)

    get_write.wait()
    pw[...] = dot(xs[...], ww[...])
    for g in range(groups):
        cols = pl.ds(g * STATE, STATE)
        for k in range(blocks):
            wrt[pl.ds(k * BLOCK, BLOCK), cols] = conv(pw, taps_w, tp * maps, cols, PAD + k * BLOCK, BLOCK).astype(BF16)

    def chain(c):
        return pltpu.make_async_remote_copy(
            src_ref=sending.at[c], dst_ref=received.at[c], send_sem=chain_send.at[c],
            recv_sem=chain_recv.at[c], device_id={"sp": following}, device_id_type=MESH,
        )

    inside = [[None] * blocks for _ in range(groups)]
    for g in range(groups):
        cols = pl.ds(g * wide, wide)
        get_value[g].wait()
        pv[:, cols] = dot(xs[...], wv[:, cols])
        lo, hi = g * wide, (g + 1) * wide
        running = None
        for k in range(blocks):
            at = pl.ds(k * BLOCK, BLOCK)
            value = conv(pv, taps_v, tp * channels, cols, PAD + k * BLOCK, BLOCK).astype(BF16)
            vals[at, cols] = value
            factor = dot(split(scale_in[:, k * BLOCK : (k + 1) * BLOCK]), expand2[:, lo:hi], ((0,), (0,)))
            scaled = (factor * value.astype(F32)).astype(BF16)
            state = dot(wrt[at, pl.ds(g * STATE, STATE)], scaled, ((0,), (0,)))
            if running is not None:
                inside[g][k] = running.astype(BF16)
                state = state + end_rows[k][:, lo:hi] * running
            running = state
        local_state[:, cols] = running
        for i in range(chunks_group):
            sending[g * chunks_group + i] = running[:, i * LANES : (i + 1) * LANES].astype(BF16)

        @pl.when(me == 0)
        def _(g=g):
            for i in range(chunks_group):
                chain(g * chunks_group + i).start()

    get_read.wait()
    pr[...] = dot(xs[...], wr[...])
    causal = (
        lax.broadcasted_iota(jnp.int32, (BLOCK, BLOCK), 0)
        >= lax.broadcasted_iota(jnp.int32, (BLOCK, BLOCK), 1)
    )
    owner = lax.broadcasted_iota(jnp.int32, (BLOCK, wide), 1) // HEAD
    for g in range(groups):
        lo, hi = g * wide, (g + 1) * wide
        cols = pl.ds(lo, wide)
        maps_at = pl.ds(g * STATE, STATE)
        for k in range(blocks):
            at = pl.ds(k * BLOCK, BLOCK)
            span = slice(k * BLOCK, (k + 1) * BLOCK)
            read = conv(pr, taps_r, tp * maps, maps_at, PAD + k * BLOCK, BLOCK).astype(BF16)
            rds[at, maps_at] = read
            scores = dot(read, wrt[at, maps_at], ((1,), (1,)))
            value = vals[at, cols]
            mixes, stacked = [], []
            for e in range(per_group):
                h = g * per_group + e
                gap = cum_cols[k][:, h : h + 1] - cums[k][h : h + 1]
                decay = jnp.exp(jnp.where(causal, gap, -jnp.inf))
                mixes.append((scores * decay * step[h : h + 1, span]).astype(BF16))
                stacked.append(jnp.where(owner == e, value, jnp.zeros_like(value)))
            y = dot(jnp.concatenate(mixes, axis=1), jnp.concatenate(stacked, axis=0))
            grown = dot(split(jnp.exp(cums[k])), expand2[:, lo:hi], ((0,), (0,)))
            if k > 0:
                y = y + grown * dot(read, inside[g][k])
            y_loc[at, cols] = y + skip_row[:, lo:hi] * value.astype(F32)
            fade[at, cols] = dot(split(jnp.exp(cums[k] + before[k])), expand2[:, lo:hi], ((0,), (0,)))
            pg[at, cols] = silu(pg[at, cols])

    base = PAD + rows
    new_value = jnp.concatenate(
        [conv(pv, taps_v, tp * channels, pl.ds(g * wide, wide), base, 1) for g in range(groups)], axis=1
    ).astype(BF16).astype(F32)
    new_write = [conv(pw, taps_w, tp * maps, pl.ds(g * STATE, STATE), base, 1).astype(BF16) for g in range(groups)]
    new_read = [conv(pr, taps_r, tp * maps, pl.ds(g * STATE, STATE), base, 1).astype(BF16) for g in range(groups)]
    new_gate = silu(pg[pl.ds(rows, 1)])
    new_decay_row = jnp.sum(expand * jnp.exp(-new_step * rates), axis=0, keepdims=True)
    new_step_row = jnp.sum(expand * new_step, axis=0, keepdims=True)

    @pl.when(me > 0)
    def _():
        for c in range(chunks):
            chain(c).wait_recv()
            at = pl.ds(c * LANES, LANES)
            state = received[c].astype(F32) * total_row[:, c * LANES : (c + 1) * LANES] + local_state[:, at]
            local_state[:, at] = state

            @pl.when(me < last)
            def _(c=c, state=state):
                sending[c] = state.astype(BF16)
                chain(c).start()

    def cache_copy(s):
        return pltpu.make_async_remote_copy(
            src_ref=cache.at[s], dst_ref=cache_out, send_sem=cache_send.at[s],
            recv_sem=cache_recv, device_id={"sp": s}, device_id_type=MESH,
        )

    def row_copy(s):
        return pltpu.make_async_remote_copy(
            src_ref=step_row, dst_ref=step_recv, send_sem=row_send.at[s],
            recv_sem=row_recv, device_id={"sp": s}, device_id_type=MESH,
        )

    own_cache = pltpu.make_async_copy(cache.at[last], cache_out, cache_recv)

    @pl.when(me == last)
    def _():
        for s in range(n):
            cache[s] = local_state[pl.ds(s * piece, piece)].astype(BF16)
        parts = []
        for g in range(groups):
            lo, hi = g * wide, (g + 1) * wide
            stored = local_state[:, pl.ds(lo, wide)].astype(BF16)
            read = jnp.broadcast_to(new_read[g], (PAD, STATE))
            fetched = dot(read, stored)[:1] * new_decay_row[:, lo:hi]
            overlap = jnp.sum(new_read[g].astype(F32) * new_write[g].astype(F32), axis=1, keepdims=True)
            value = new_value[:, lo:hi]
            mixed = fetched + new_step_row[:, lo:hi] * overlap * value + skip_row[:, lo:hi] * value
            gated = mixed * new_gate[:, lo:hi]
            mean = jnp.sum(gated * gated, axis=1, keepdims=True) * (1.0 / wide)
            parts.append(gated * lax.rsqrt(mean + EPSILON) * gain_row[:, lo:hi])
        row = jnp.broadcast_to(jnp.concatenate(parts, axis=1), (8, channels))
        step_row[...] = row
        step_recv[...] = row
        for s in range(last):
            cache_copy(s).start()
            row_copy(s).start()
        own_cache.start()

    def finish(k, g, arrived):
        at = pl.ds(k * BLOCK, BLOCK)
        cols = pl.ds(g * wide, wide)
        y = y_loc[at, cols]
        if arrived is not None:
            y = y + fade[at, cols] * dot(rds[at, pl.ds(g * STATE, STATE)], arrived)
        gated = y * pg[at, cols]
        mean = jnp.sum(gated * gated, axis=1, keepdims=True) * (1.0 / wide)
        normed = gated * lax.rsqrt(mean + EPSILON) * gain_row[:, g * wide : (g + 1) * wide]
        result[at, cols] = normed.astype(BF16)

    @pl.when(me == 0)
    def _():
        received[...] = jnp.zeros(received.shape, BF16)

    writes = []
    for g in range(groups):
        arrived = jnp.concatenate([received[g * chunks_group + i] for i in range(chunks_group)], axis=1)
        for k in range(blocks):
            finish(k, g, arrived)
    for k in range(blocks):
        at = pl.ds(k * BLOCK, BLOCK)
        copy = pltpu.make_async_copy(result.at[at], out.at[at], out_sem.at[k])
        copy.start()
        writes.append(copy)

    @pl.when(me < last)
    def _():
        for c in range(chunks):
            chain(c).wait_send()
        halo.wait_send()
        row_copy(0).wait_recv()
        cache_copy(0).wait_recv()

    columns = channels // n
    mine = lax.broadcasted_iota(jnp.int32, (8, channels), 1) % n == me
    picked = jnp.where(mine, step_recv[...], 0.0).astype(BF16)
    choose = (
        lax.broadcasted_iota(jnp.int32, (channels, columns), 0) // n
        == lax.broadcasted_iota(jnp.int32, (channels, columns), 1)
    ).astype(F32).astype(BF16)
    step_out[...] = dot(picked, choose)[:1].astype(BF16)

    @pl.when(me == last)
    def _():
        for s in range(last):
            cache_copy(s).wait_send()
            row_copy(s).wait_send()
        own_cache.wait()

    for copy in writes:
        copy.wait()


def on_device(
    tokens, fresh, w_value, w_write, w_read, w_gate, step_matrix, taps_v, taps_w, taps_r,
    log_rate, offset_bias, spike, bypass, gain,
):
    n = lax.axis_size("sp")
    rows, width = tokens.shape
    channels = w_value.shape[1]
    maps = w_write.shape[1]
    groups = maps // STATE
    chunks = channels // LANES
    blocks = rows // BLOCK
    piece = STATE // n
    any_space = pl.BlockSpec(memory_space=pl.ANY)
    vmem = pl.BlockSpec(memory_space=pltpu.VMEM)
    dma = pltpu.SemaphoreType.DMA
    out, cache, step = pl.pallas_call(
        functools.partial(kernel, n),
        out_shape=(
            jax.ShapeDtypeStruct((rows, channels), BF16),
            jax.ShapeDtypeStruct((piece, channels), BF16),
            jax.ShapeDtypeStruct((1, channels // n), BF16),
        ),
        in_specs=[any_space, vmem, any_space, any_space, any_space, any_space] + [vmem] * 9,
        out_specs=(any_space, any_space, vmem),
        scratch_shapes=[
            pltpu.VMEM((rows + 2 * PAD, width), BF16),
            pltpu.VMEM((width, channels), BF16),
            pltpu.VMEM((width, maps), BF16),
            pltpu.VMEM((width, maps), BF16),
            pltpu.VMEM((width, channels), BF16),
            pltpu.VMEM((rows + 2 * PAD, channels), F32),
            pltpu.VMEM((rows + 2 * PAD, maps), F32),
            pltpu.VMEM((rows + 2 * PAD, maps), F32),
            pltpu.VMEM((rows + PAD, channels), F32),
            pltpu.VMEM((step_matrix.shape[1], rows), F32),
            pltpu.VMEM((rows, channels), BF16),
            pltpu.VMEM((rows, maps), BF16),
            pltpu.VMEM((rows, maps), BF16),
            pltpu.VMEM((rows, channels), F32),
            pltpu.VMEM((rows, channels), F32),
            pltpu.VMEM((STATE, channels), F32),
            pltpu.VMEM((chunks, STATE, LANES), BF16),
            pltpu.VMEM((chunks, STATE, LANES), BF16),
            pltpu.VMEM((n, piece, channels), BF16),
            pltpu.VMEM((8, channels), F32),
            pltpu.VMEM((8, channels), F32),
            pltpu.VMEM((rows, channels), BF16),
            dma((3 + 2 * groups,)),
            dma, dma,
            dma((chunks,)), dma((chunks,)),
            dma((n,)), dma, dma((n,)), dma,
            dma((blocks,)),
        ],
        compiler_params=pltpu.CompilerParams(collective_id=0, has_side_effects=True),
    )(
        tokens, fresh.reshape(width // LANES, LANES), w_value, w_write, w_read, w_gate, step_matrix.T,
        taps_v, taps_w, taps_r, log_rate[None], offset_bias[None], spike.T, bypass[None],
        gain.reshape(-1, LANES),
    )
    return (out, cache, step.T)


def solution(mesh):
    placed = (
        P(("grp", "sp"), None), P("grp"), P(None, "tp"), P(None, "tp"), P(None, "tp"), P(None, "tp"),
        P(), P(), P(), P(), P(), P(), P(("grp", "sp"), "tp"), P(), P(),
    )
    return jax.shard_map(
        on_device,
        mesh=mesh,
        in_specs=placed,
        out_specs=(P(("grp", "sp"), "tp"), P(("grp", "sp"), "tp"), P(("grp", "tp"), "sp")),
        check_vma=False,
    )
```

time: 127 us -> 35.8 us (0.28)
  Pallas kernels: 0 us -> 30.5 us
  blocking collectives: 30.3 us -> 0 us
  local copies, waits for them, and re-layouts: 28.8 us -> 4.39 us
  matrix products: 22.6 us -> 0 us
  other arithmetic: 20.4 us -> 0 us
  starting transfers between devices: 19.8 us -> 0 us
  waiting for transfers between devices: 3.3 us -> 0 us
    pallas_call x0 -> x1, Pallas kernels: none -> 30.5 us  [on_device(): pl.pallas_call(functools.partial(kernel, n), out_shape=(jax.ShapeDtypeStr...]
    psum x2 -> x0, blocking collectives: 22.7 us -> none  [the longest x1 12.2 us: on_device(): reading = lax.psum(partial_value, 'sp')]
    dot_general x17 -> x0, matrix products: 22.6 us -> none  [the longest x8 12.6 us: project(): jnp.dot(operand, weights, preferred_element_type=jnp.float32)]
    ppermute x3 -> x0, starting transfers between devices: 12.8 us -> none  [passed_along(): return lax.ppermute(block, axis, route)]
    reshape x10 -> x0, local copies, waits for them, and re-layouts: 8.8 us -> none  [the longest x2 5.28 us: on_device(): (inner_part + carried_part).reshape(row_count, head_count, HEAD)]
    convert_element_type x15 -> x0, other arithmetic: 8.78 us -> none  [the longest x5 2.36 us: apply_taps(): joined = jnp.concatenate([previous, current], axis=0).astype(jnp.float32)]
    all_gather x1 -> x0, blocking collectives: 7.58 us -> none  [on_device(): lax.all_gather(shard_fading_factor[None], 'sp', axis=0, tiled=True)]
    all_to_all x2 -> x0, starting transfers between devices: 7.02 us -> none  [the longest x1 3.58 us: on_device(): lax.all_to_all(running[None], 'sp', split_axis=1, concat_axis=0, tiled=True)]
  transfers between devices with their start and end apart: 5 -> 0, of which waited for: 1 -> 0; matrix products, arithmetic and copies ran while one was open for 26% -> 0% of each run, Pallas kernels for 0% -> 0%
where the time goes in v1:
time: 35.8 us; the launch traced here: 35.5 us
  Pallas kernels  30.5 us (85%)
  local copies, waits for them, and re-layouts  4.39 us (12%)
  between operations  0.65 us (2%)
    pallas_call x1, Pallas kernels, on_device(): pl.pallas_call(functools.partial(kernel, n), out_shape=(jax.ShapeDtypeStr...  30.5 us
    unnamed x3, local copies, waits for them, and re-layouts  4.39 us

profile of v1, /device:TPU:0, one launch (start us, length us, event | category | flops | bytes accessed | tf_op | source)
XLA Modules:
  0.0 35.5 jit_solution(8783930972231142279)
XLA Ops:
  0.6 30.5 %shard_map.166 = (bf16[512,512]{1,0:T(8,128)(2,1)}, bf16[32,512]{1,0:T(8,128)(2,1)}, bf16[1,128]{1,0:T(2,128)(2,1)}) custom-call(bf16[512,2048]{1,0:T(8,128)(2,1)} %tokens.1, bf16[16,128]{1,0:T(8,128)(2,1)} %bitcast.11, bf16[2048,512]{1,0:T(8,128)(2,1)} %w_value.1, bf16[2048,256]{1,0:T(8,128)(2,1)} %w_write.1, bf16[2048,256]{1,0:T(8,128)(2,1)} %w_read.1, ...), custom_call_target="tpu_custom_call" | custom-call | tf_op jit(solution)/shard_map/pallas_call | solution.py:378
  31.1 1.9 %copy.21 = bf16[512,512]{1,0:T(8,128)(2,1)} copy(bf16[512,512]{1,0:T(8,128)(2,1)} %get-tuple-element.12) | data formatting | bytes 1048576
  33.0 1.4 %copy.22 = bf16[32,512]{1,0:T(8,128)(2,1)} copy(bf16[32,512]{1,0:T(8,128)(2,1)} %get-tuple-element.13) | data formatting | bytes 65536
  34.4 1.1 %copy.23 = bf16[128,1]{0,1:T(2,128)(2,1)} copy(bf16[128,1]{0,1:T(2,128)(2,1)} %bitcast.15) | data formatting | bytes 512

commit v2 on v1

--- a/solution.py
+++ b/solution.py
@@ -38,13 +38,14 @@
 
 
 def kernel(
-    n, tokens, fresh, w_value, w_write, w_read, w_gate, step_t, taps_v, taps_w, taps_r,
-    log_rate, offset_bias, spike_t, bypass, gain,
-    out, cache_out, step_out,
+    n, tokens, fresh_hbm, w_value, w_write, w_read, w_gate, step_hbm, taps_v_hbm, taps_w_hbm, taps_r_hbm,
+    log_rate_hbm, bias_hbm, spike_hbm, bypass_hbm, gain_hbm,
+    result, cache_in, step_out,
+    fresh, step_t, taps_v, taps_w, taps_r, log_rate, offset_bias, spike_t, bypass, gain,
     xs, wv, ww, wr, wg, pv, pw, pr, pg, raw_t, vals, wrt, rds, y_loc, fade, local_state,
-    received, sending, cache, step_row, step_recv, result,
+    received, sending, cache, step_row, step_recv,
     load_sem, halo_send, halo_recv, chain_send, chain_recv, cache_send, cache_recv,
-    row_send, row_recv, out_sem,
+    row_send, row_recv, small_sem,
 ):
     rows, width = tokens.shape
     channels = w_value.shape[1]
@@ -70,18 +71,28 @@
         copy.start()
         return copy
 
+    barrier = pltpu.get_barrier_semaphore()
+
+    @pl.when(me > 0)
+    def _():
+        pl.semaphore_signal(barrier, inc=1, device_id={"sp": me - 1}, device_id_type=MESH)
+
+    small = [
+        pltpu.make_async_copy(src, dst, small_sem.at[i])
+        for i, (src, dst) in enumerate((
+            (fresh_hbm, fresh), (step_hbm, step_t), (taps_v_hbm, taps_v), (taps_w_hbm, taps_w),
+            (taps_r_hbm, taps_r), (log_rate_hbm, log_rate), (bias_hbm, offset_bias),
+            (spike_hbm, spike_t), (bypass_hbm, bypass), (gain_hbm, gain),
+        ))
+    ]
     get_tokens = load(tokens, xs.at[pl.ds(PAD, rows)])
+    for copy in small:
+        copy.start()
     get_gate = [load(w_gate.at[:, pl.ds(g * wide, wide)], wg.at[:, pl.ds(g * wide, wide)]) for g in range(groups)]
     get_write = load(w_write, ww)
     get_value = [load(w_value.at[:, pl.ds(g * wide, wide)], wv.at[:, pl.ds(g * wide, wide)]) for g in range(groups)]
     get_read = load(w_read, wr)
 
-    barrier = pltpu.get_barrier_semaphore()
-
-    @pl.when(me > 0)
-    def _():
-        pl.semaphore_signal(barrier, inc=1, device_id={"sp": me - 1}, device_id_type=MESH)
-
     @pl.when(me < last)
     def _():
         pl.semaphore_wait(barrier, 1)
@@ -95,6 +106,9 @@
     @pl.when(me < last)
     def _():
         halo.start()
+
+    for copy in small:
+        copy.wait()
 
     fresh_f = fresh[...].astype(F32)
     fresh_row = jnp.concatenate([fresh_f[i : i + 1] for i in range(width // LANES)], axis=1)
@@ -255,23 +269,10 @@
     new_decay_row = jnp.sum(expand * jnp.exp(-new_step * rates), axis=0, keepdims=True)
     new_step_row = jnp.sum(expand * new_step, axis=0, keepdims=True)
 
-    @pl.when(me > 0)
-    def _():
-        for c in range(chunks):
-            chain(c).wait_recv()
-            at = pl.ds(c * LANES, LANES)
-            state = received[c].astype(F32) * total_row[:, c * LANES : (c + 1) * LANES] + local_state[:, at]
-            local_state[:, at] = state
-
-            @pl.when(me < last)
-            def _(c=c, state=state):
-                sending[c] = state.astype(BF16)
-                chain(c).start()
-
-    def cache_copy(s):
+    def cache_copy(s, c):
         return pltpu.make_async_remote_copy(
-            src_ref=cache.at[s], dst_ref=cache_out, send_sem=cache_send.at[s],
-            recv_sem=cache_recv, device_id={"sp": s}, device_id_type=MESH,
+            src_ref=cache.at[c, s], dst_ref=cache_in.at[c], send_sem=cache_send.at[c, s],
+            recv_sem=cache_recv.at[c], device_id={"sp": s}, device_id_type=MESH,
         )
 
     def row_copy(s):
@@ -280,12 +281,29 @@
             recv_sem=row_recv, device_id={"sp": s}, device_id_type=MESH,
         )
 
-    own_cache = pltpu.make_async_copy(cache.at[last], cache_out, cache_recv)
+    @pl.when(me > 0)
+    def _():
+        for c in range(chunks):
+            chain(c).wait_recv()
+            at = pl.ds(c * LANES, LANES)
+            state = received[c].astype(F32) * total_row[:, c * LANES : (c + 1) * LANES] + local_state[:, at]
+
+            @pl.when(me < last)
+            def _(c=c, state=state):
+                sending[c] = state.astype(BF16)
+                chain(c).start()
+
+            @pl.when(me == last)
+            def _(c=c, state=state, at=at):
+                local_state[:, at] = state
+                for s in range(n):
+                    cache[c, s] = state[s * piece : (s + 1) * piece].astype(BF16)
+                cache_in[c] = state[last * piece :].astype(BF16)
+                for s in range(last):
+                    cache_copy(s, c).start()
 
     @pl.when(me == last)
     def _():
-        for s in range(n):
-            cache[s] = local_state[pl.ds(s * piece, piece)].astype(BF16)
         parts = []
         for g in range(groups):
             lo, hi = g * wide, (g + 1) * wide
@@ -298,13 +316,12 @@
             gated = mixed * new_gate[:, lo:hi]
             mean = jnp.sum(gated * gated, axis=1, keepdims=True) * (1.0 / wide)
             parts.append(gated * lax.rsqrt(mean + EPSILON) * gain_row[:, lo:hi])
-        row = jnp.broadcast_to(jnp.concatenate(parts, axis=1), (8, channels))
-        step_row[...] = row
-        step_recv[...] = row
+        for c in range(chunks):
+            row = parts[c // chunks_group][:, (c % chunks_group) * LANES : (c % chunks_group + 1) * LANES]
+            step_row[pl.ds(c, 1)] = row
+            step_recv[pl.ds(c, 1)] = row
         for s in range(last):
-            cache_copy(s).start()
             row_copy(s).start()
-        own_cache.start()
 
     def finish(k, g, arrived):
         at = pl.ds(k * BLOCK, BLOCK)
@@ -321,16 +338,10 @@
     def _():
         received[...] = jnp.zeros(received.shape, BF16)
 
-    writes = []
     for g in range(groups):
         arrived = jnp.concatenate([received[g * chunks_group + i] for i in range(chunks_group)], axis=1)
         for k in range(blocks):
             finish(k, g, arrived)
-    for k in range(blocks):
-        at = pl.ds(k * BLOCK, BLOCK)
-        copy = pltpu.make_async_copy(result.at[at], out.at[at], out_sem.at[k])
-        copy.start()
-        writes.append(copy)
 
     @pl.when(me < last)
     def _():
@@ -338,11 +349,13 @@
             chain(c).wait_send()
         halo.wait_send()
         row_copy(0).wait_recv()
-        cache_copy(0).wait_recv()
+        for c in range(chunks):
+            cache_copy(0, c).wait_recv()
 
     columns = channels // n
     mine = lax.broadcasted_iota(jnp.int32, (8, channels), 1) % n == me
-    picked = jnp.where(mine, step_recv[...], 0.0).astype(BF16)
+    whole = jnp.concatenate([step_recv[pl.ds(c, 1)] for c in range(chunks)], axis=1)
+    picked = jnp.where(mine, jnp.broadcast_to(whole, (8, channels)), 0.0).astype(BF16)
     choose = (
         lax.broadcasted_iota(jnp.int32, (channels, columns), 0) // n
         == lax.broadcasted_iota(jnp.int32, (channels, columns), 1)
@@ -352,11 +365,21 @@
     @pl.when(me == last)
     def _():
         for s in range(last):
-            cache_copy(s).wait_send()
             row_copy(s).wait_send()
-        own_cache.wait()
-
-    for copy in writes:
+            for c in range(chunks):
+                cache_copy(s, c).wait_send()
+
+
+def deliver(result, cache_in, step, out, cache_out, step_out, sems):
+    copies = [
+        pltpu.make_async_copy(result, out, sems.at[0]),
+        pltpu.make_async_copy(step, step_out, sems.at[1]),
+    ]
+    for c in range(cache_in.shape[0]):
+        copies.append(pltpu.make_async_copy(cache_in.at[c], cache_out.at[:, pl.ds(c * LANES, LANES)], sems.at[2 + c]))
+    for copy in copies:
+        copy.start()
+    for copy in copies:
         copy.wait()
 
 
@@ -370,21 +393,32 @@
     maps = w_write.shape[1]
     groups = maps // STATE
     chunks = channels // LANES
-    blocks = rows // BLOCK
     piece = STATE // n
     any_space = pl.BlockSpec(memory_space=pl.ANY)
     vmem = pl.BlockSpec(memory_space=pltpu.VMEM)
     dma = pltpu.SemaphoreType.DMA
-    out, cache, step = pl.pallas_call(
+    heads = channels // HEAD
+    all_heads = step_matrix.shape[1]
+    passed = pl.pallas_call(
         functools.partial(kernel, n),
         out_shape=(
-            jax.ShapeDtypeStruct((rows, channels), BF16),
-            jax.ShapeDtypeStruct((piece, channels), BF16),
-            jax.ShapeDtypeStruct((1, channels // n), BF16),
+            pltpu.VMEM((rows, channels), BF16),
+            pltpu.VMEM((chunks, piece, LANES), BF16),
+            pltpu.VMEM((1, channels // n), BF16),
         ),
-        in_specs=[any_space, vmem, any_space, any_space, any_space, any_space] + [vmem] * 9,
-        out_specs=(any_space, any_space, vmem),
+        in_specs=[any_space] * 15,
+        out_specs=(vmem, vmem, vmem),
         scratch_shapes=[
+            pltpu.VMEM((width // LANES, LANES), BF16),
+            pltpu.VMEM((all_heads, width), BF16),
+            pltpu.VMEM(taps_v.shape, BF16),
+            pltpu.VMEM(taps_w.shape, BF16),
+            pltpu.VMEM(taps_r.shape, BF16),
+            pltpu.VMEM((1, all_heads), F32),
+            pltpu.VMEM((1, all_heads), F32),
+            pltpu.VMEM((heads, rows), F32),
+            pltpu.VMEM((1, all_heads), F32),
+            pltpu.VMEM((gain.shape[0] // LANES, LANES), F32),
             pltpu.VMEM((rows + 2 * PAD, width), BF16),
             pltpu.VMEM((width, channels), BF16),
             pltpu.VMEM((width, maps), BF16),
@@ -403,15 +437,14 @@
             pltpu.VMEM((STATE, channels), F32),
             pltpu.VMEM((chunks, STATE, LANES), BF16),
             pltpu.VMEM((chunks, STATE, LANES), BF16),
-            pltpu.VMEM((n, piece, channels), BF16),
-            pltpu.VMEM((8, channels), F32),
-            pltpu.VMEM((8, channels), F32),
-            pltpu.VMEM((rows, channels), BF16),
+            pltpu.VMEM((chunks, n, piece, LANES), BF16),
+            pltpu.VMEM((8, LANES), F32),
+            pltpu.VMEM((8, LANES), F32),
             dma((3 + 2 * groups,)),
             dma, dma,
             dma((chunks,)), dma((chunks,)),
-            dma((n,)), dma, dma((n,)), dma,
-            dma((blocks,)),
+            dma((chunks, n)), dma((chunks,)), dma((n,)), dma,
+            dma((10,)),
         ],
         compiler_params=pltpu.CompilerParams(collective_id=0, has_side_effects=True),
     )(
@@ -419,6 +452,17 @@
         taps_v, taps_w, taps_r, log_rate[None], offset_bias[None], spike.T, bypass[None],
         gain.reshape(-1, LANES),
     )
+    out, cache, step = pl.pallas_call(
+        deliver,
+        out_shape=(
+            jax.ShapeDtypeStruct((rows, channels), BF16),
+            jax.ShapeDtypeStruct((piece, channels), BF16),
+            jax.ShapeDtypeStruct((1, channels // n), BF16),
+        ),
+        in_specs=[vmem] * 3,
+        out_specs=(any_space,) * 3,
+        scratch_shapes=[dma((2 + chunks,))],
+    )(*(pltpu.with_memory_space_constraint(x, pltpu.VMEM) for x in passed))
     return (out, cache, step.T)
 
 

time: 35.8 us -> 32 us (0.89)
  local copies, waits for them, and re-layouts: 4.39 us -> 0 us
  Pallas kernels: 30.5 us -> 31.2 us
    unnamed x3 -> x0, local copies, waits for them, and re-layouts: 4.39 us -> none
    pallas_call x1 -> x2, Pallas kernels: 30.5 us -> 31.2 us  [the longest x1 30.3 us: on_device(): pl.pallas_call(functools.partial(kernel, n), out_shape=(pltpu.VMEM((rows,...]
where the time goes in v2:
time: 32 us; the launch traced here: 31.8 us
  Pallas kernels  31.2 us (98%)
  between operations  0.64 us (2%)
    pallas_call x1, Pallas kernels, on_device(): pl.pallas_call(functools.partial(kernel, n), out_shape=(pltpu.VMEM((rows,...  30.3 us
    pallas_call x1, Pallas kernels, on_device(): pl.pallas_call(deliver, out_shape=(jax.ShapeDtypeStruct((rows, channels),...  0.86 us

profile of v2, /device:TPU:0, one launch (start us, length us, event | category | flops | bytes accessed | tf_op | source)
XLA Modules:
  0.0 31.8 jit_solution(4009490294780042442)
XLA Ops:
  0.6 30.3 %shard_map.166 = (bf16[512,512]{1,0:T(8,128)(2,1)S(1)}, bf16[4,32,128]{2,1,0:T(8,128)(2,1)S(1)}, bf16[1,128]{1,0:T(2,128)(2,1)S(1)}) custom-call(bf16[512,2048]{1,0:T(8,128)(2,1)} %tokens.1, bf16[16,128]{1,0:T(8,128)(2,1)} %bitcast.11, bf16[2048,512]{1,0:T(8,128)(2,1)} %w_value.1, bf16[2048,256]{1,0:T(8,128)(2,1)} %w_write.1, bf16[2048,256]{1,0:T(8,128)(2,1)} %w_read.1, ...), custom_call_target="tpu_custom_call" | custom-call | tf_op jit(solution)/shard_map/pallas_call | solution.py:402
  31.0 0.9 %shard_map.167 = (bf16[512,512]{1,0:T(8,128)(2,1)}, bf16[32,512]{1,0:T(8,128)(2,1)}, bf16[1,128]{1,0:T(2,128)(2,1)}) custom-call(bf16[512,512]{1,0:T(8,128)(2,1)S(1)} %get-tuple-element.9.result, bf16[4,32,128]{2,1,0:T(8,128)(2,1)S(1)} %get-tuple-element.10.cache_in, bf16[1,128]{1,0:T(2,128)(2,1)S(1)} %get-tuple-element.11.step), custom_call_target="tpu_custom_call" | custom-call | tf_op jit(solution)/shard_map/pallas_call | solution.py:455

commit v3 on v2

--- a/solution.py
+++ b/solution.py
@@ -13,6 +13,7 @@
 BLOCK = 128
 PAD = 16
 LANES = 128
+CUTS = 2
 EPSILON = 1e-06
 F32 = jnp.float32
 BF16 = jnp.bfloat16
@@ -168,11 +169,6 @@
     end_rows = [jnp.sum(expand * jnp.exp(e), axis=0, keepdims=True) for e in ends]
     total_row = jnp.sum(expand * jnp.exp(before[blocks]), axis=0, keepdims=True)
 
-    for g in range(groups):
-        cols = pl.ds(g * wide, wide)
-        get_gate[g].wait()
-        pg[:, cols] = dot(xs[pl.ds(PAD, rows + PAD)], wg[:, cols])
-
     @pl.when(me > 0)
     def _():
         halo.wait_recv()
@@ -193,10 +189,11 @@
         for k in range(blocks):
             wrt[pl.ds(k * BLOCK, BLOCK), cols] = conv(pw, taps_w, tp * maps, cols, PAD + k * BLOCK, BLOCK).astype(BF16)
 
-    def chain(c):
+    def chain(c, part):
+        at = pl.ds(part * (STATE // CUTS), STATE // CUTS)
         return pltpu.make_async_remote_copy(
-            src_ref=sending.at[c], dst_ref=received.at[c], send_sem=chain_send.at[c],
-            recv_sem=chain_recv.at[c], device_id={"sp": following}, device_id_type=MESH,
+            src_ref=sending.at[c, at], dst_ref=received.at[c, at], send_sem=chain_send.at[c, part],
+            recv_sem=chain_recv.at[c, part], device_id={"sp": following}, device_id_type=MESH,
         )
 
     inside = [[None] * blocks for _ in range(groups)]
@@ -224,7 +221,13 @@
         @pl.when(me == 0)
         def _(g=g):
             for i in range(chunks_group):
-                chain(g * chunks_group + i).start()
+                for part in range(CUTS):
+                    chain(g * chunks_group + i, part).start()
+
+    for g in range(groups):
+        cols = pl.ds(g * wide, wide)
+        get_gate[g].wait()
+        pg[:, cols] = dot(xs[pl.ds(PAD, rows + PAD)], wg[:, cols])
 
     get_read.wait()
     pr[...] = dot(xs[...], wr[...])
@@ -284,18 +287,22 @@
     @pl.when(me > 0)
     def _():
         for c in range(chunks):
-            chain(c).wait_recv()
             at = pl.ds(c * LANES, LANES)
-            state = received[c].astype(F32) * total_row[:, c * LANES : (c + 1) * LANES] + local_state[:, at]
-
-            @pl.when(me < last)
-            def _(c=c, state=state):
-                sending[c] = state.astype(BF16)
-                chain(c).start()
+            for part in range(CUTS):
+                chain(c, part).wait_recv()
+                span = pl.ds(part * (STATE // CUTS), STATE // CUTS)
+                local_state[span, at] = (
+                    received[c, span].astype(F32) * total_row[:, c * LANES : (c + 1) * LANES] + local_state[span, at]
+                )
+
+                @pl.when(me < last)
+                def _(c=c, part=part, span=span, at=at):
+                    sending[c, span] = local_state[span, at].astype(BF16)
+                    chain(c, part).start()
 
             @pl.when(me == last)
-            def _(c=c, state=state, at=at):
-                local_state[:, at] = state
+            def _(c=c, at=at):
+                state = local_state[:, at]
                 for s in range(n):
                     cache[c, s] = state[s * piece : (s + 1) * piece].astype(BF16)
                 cache_in[c] = state[last * piece :].astype(BF16)
@@ -346,7 +353,8 @@
     @pl.when(me < last)
     def _():
         for c in range(chunks):
-            chain(c).wait_send()
+            for part in range(CUTS):
+                chain(c, part).wait_send()
         halo.wait_send()
         row_copy(0).wait_recv()
         for c in range(chunks):
@@ -442,7 +450,7 @@
             pltpu.VMEM((8, LANES), F32),
             dma((3 + 2 * groups,)),
             dma, dma,
-            dma((chunks,)), dma((chunks,)),
+            dma((chunks, CUTS)), dma((chunks, CUTS)),
             dma((chunks, n)), dma((chunks,)), dma((n,)), dma,
             dma((10,)),
         ],

time: 32 us -> 31.9 us (level)
  no operation moved by 1% of the time
where the time goes in v3:
time: 31.9 us; the launch traced here: 31.8 us
  Pallas kernels  31.1 us (97%)
  between operations  0.64 us (2%)
    pallas_call x1, Pallas kernels, on_device(): pl.pallas_call(functools.partial(kernel, n), out_shape=(pltpu.VMEM((rows,...  30.3 us
    pallas_call x1, Pallas kernels, on_device(): pl.pallas_call(deliver, out_shape=(jax.ShapeDtypeStruct((rows, channels),...  0.86 us

profile of v3, /device:TPU:0, one launch (start us, length us, event | category | flops | bytes accessed | tf_op | source)
XLA Modules:
  0.0 31.8 jit_solution(16024668198593189516)
XLA Ops:
  0.6 30.3 %shard_map.166 = (bf16[512,512]{1,0:T(8,128)(2,1)S(1)}, bf16[4,32,128]{2,1,0:T(8,128)(2,1)S(1)}, bf16[1,128]{1,0:T(2,128)(2,1)S(1)}) custom-call(bf16[512,2048]{1,0:T(8,128)(2,1)} %tokens.1, bf16[16,128]{1,0:T(8,128)(2,1)} %bitcast.11, bf16[2048,512]{1,0:T(8,128)(2,1)} %w_value.1, bf16[2048,256]{1,0:T(8,128)(2,1)} %w_write.1, bf16[2048,256]{1,0:T(8,128)(2,1)} %w_read.1, ...), custom_call_target="tpu_custom_call" | custom-call | tf_op jit(solution)/shard_map/pallas_call | solution.py:410
  30.9 0.9 %shard_map.167 = (bf16[512,512]{1,0:T(8,128)(2,1)}, bf16[32,512]{1,0:T(8,128)(2,1)}, bf16[1,128]{1,0:T(2,128)(2,1)}) custom-call(bf16[512,512]{1,0:T(8,128)(2,1)S(1)} %get-tuple-element.9.result, bf16[4,32,128]{2,1,0:T(8,128)(2,1)S(1)} %get-tuple-element.10.cache_in, bf16[1,128]{1,0:T(2,128)(2,1)S(1)} %get-tuple-element.11.step), custom_call_target="tpu_custom_call" | custom-call | tf_op jit(solution)/shard_map/pallas_call | solution.py:463
